TPU v7x, 128 devices: a whole 4x4x4 slice. The times are simulated.
128 devices in a mesh: ra: 16 (over z, x), cb: 8 (over y, core).
Axes of the slice: x: 4, y: 4, z: 4, core: 2. Of those that a mesh axis runs over, the one named last changes fastest.
Arguments:
- tokens: bfloat16 [512, 3072], P(None, 'ra'), may hold values from -14 to 14
- norm_gain: float32 [2, 3072], P(None, 'ra'), may hold values from 0.1 to 1.9
- gate_weight: float32 [2, 3072, 8448], P(None, 'ra', 'cb'), may hold values from -0.109375 to 0.109375
- gate_scale: float32 [2, 8448], P(None, 'cb'), may hold values from 0.5 to 2
- value_weight: float32 [2, 3072, 8448], P(None, 'ra', 'cb'), may hold values from -0.109375 to 0.109375
- value_scale: float32 [2, 8448], P(None, 'cb'), may hold values from 0.5 to 2
- gate_conv: float32 [2, 3, 8448], P(None, None, 'cb'), may hold values from -3.5 to 3.5
- value_conv: float32 [2, 3, 8448], P(None, None, 'cb'), may hold values from -3.5 to 3.5
- gate_bias: float32 [2, 8448], P(None, 'cb'), may hold values from -3 to 3
- value_bias: float32 [2, 8448], P(None, 'cb'), may hold values from -3 to 3
- down_weight: float32 [2, 8448, 3072], P(None, 'cb', 'ra'), may hold values from -0.0625 to 0.0625
- down_scale: float32 [2, 3072], P(None, 'ra'), may hold values from 0.5 to 2
Outputs:
- stream_out: bfloat16 [512, 3072], P(None, 'ra')
All inputs are finite; a program needn't handle non-finite values.
Results may differ from a plain program's by a relative error of at most 0.039.
Values may be sent and summed in bfloat16 or wider, within the bound.
A program may use at most 64 MiB of HBM per device.

v0:
```python
import jax
import jax.numpy as jnp
from jax import lax
from jax.sharding import PartitionSpec as P

D = 3072
TAPS = 3
LAYERS = 2
SEQ_LEN = 8


epsilon = 1e-06
residual_keep = 0.5


def copy_for_each(array, axis):
    copies = jnp.broadcast_to(array, (lax.axis_size(axis), *array.shape))
    return lax.all_to_all(copies, axis, split_axis=0, concat_axis=0, tiled=True)


def taken_together(array, axis):
    return copy_for_each(array, axis).astype(jnp.float32).sum(axis=0)


def causal_conv(values, conv_taps, conv_bias):
    row_count, col_count = values.shape
    blocks = values.reshape(row_count // SEQ_LEN, SEQ_LEN, col_count)
    padded = jnp.pad(blocks, ((0, 0), (TAPS - 1, 0), (0, 0)))
    summed = conv_bias + jnp.zeros_like(blocks)
    for offset in range(TAPS):
        summed = summed + padded[:, offset : offset + SEQ_LEN] * conv_taps[offset]
    return summed.reshape(row_count, col_count)


def shards(
    tokens,
    norm_gain,
    gate_weight,
    gate_scale,
    value_weight,
    value_scale,
    gate_conv,
    value_conv,
    gate_bias,
    value_bias,
    down_weight,
    down_scale,
):
    stream = tokens
    for depth_index in range(LAYERS):
        widened = stream.astype(jnp.float32)
        local_squares = jnp.sum(widened * widened, axis=1)
        normed = (widened * norm_gain[depth_index]).astype(jnp.bfloat16)
        gate_part = jnp.dot(
            normed,
            gate_weight[depth_index].astype(jnp.bfloat16),
            preferred_element_type=jnp.float32,
        )
        value_part = jnp.dot(
            normed,
            value_weight[depth_index].astype(jnp.bfloat16),
            preferred_element_type=jnp.float32,
        )
        squares, gate_pre, value_pre = (
            lax.psum(local_squares.astype(jnp.bfloat16), "ra").astype(jnp.float32),
            lax.psum(gate_part.astype(jnp.bfloat16), "ra").astype(jnp.float32),
            lax.psum(value_part.astype(jnp.bfloat16), "ra").astype(jnp.float32),
        )
        inverse_rms = lax.rsqrt(squares / D + epsilon)[:, None]
        gate_mixed = causal_conv(
            gate_pre * inverse_rms * gate_scale[depth_index],
            gate_conv[depth_index],
            gate_bias[depth_index],
        )
        value_mixed = causal_conv(
            value_pre * inverse_rms * value_scale[depth_index],
            value_conv[depth_index],
            value_bias[depth_index],
        )
        hidden = (jax.nn.silu(gate_mixed) * value_mixed).astype(jnp.bfloat16)
        partial_value = jnp.dot(
            hidden,
            down_weight[depth_index].astype(jnp.bfloat16),
            preferred_element_type=jnp.float32,
        )
        branch = (
            taken_together(partial_value.astype(jnp.bfloat16), "cb").astype(jnp.float32)
            * down_scale[depth_index]
        )
        stream = (residual_keep * widened + branch).astype(jnp.bfloat16)
    return stream


def solution(mesh):
    placed = (
        P(None, "ra"),
        P(None, "ra"),
        P(None, "ra", "cb"),
        P(None, "cb"),
        P(None, "ra", "cb"),
        P(None, "cb"),
        P(None, None, "cb"),
        P(None, None, "cb"),
        P(None, "cb"),
        P(None, "cb"),
        P(None, "cb", "ra"),
        P(None, "ra"),
    )
    return jax.shard_map(
        shards, mesh=mesh, in_specs=placed, out_specs=P(None, "ra"), check_vma=False
    )
```

profile of v0, /device:TPU:1, one launch (start us, length us, event | category | flops | bytes accessed | tf_op | source)
XLA Modules:
  0.0 293.0 jit_solution(3064619238988429749)
XLA Ops:
  6.5 0.0 all-reduce.11.cloned.1.call-start
  6.5 1.4 fusion.54
  7.9 1.6 convert.13
  9.5 0.0 copy-done.5
  9.6 0.1 convert.12
  9.7 0.0 copy-start
  9.7 0.0 copy-done.2
  9.7 1.6 convolution_convert_fusion.2
  11.3 0.0 copy-done
  11.3 1.6 convolution_convert_fusion.3
  12.9 0.0 copy-start.8
  12.9 0.0 copy-start.9
  12.9 0.0 all-reduce.11.cloned.1.call-update
  12.9 0.0 copy-done.6
  12.9 1.0 convert.14
  14.0 0.1 fusion.39
  14.0 35.7 %psum.43 = bf16[512]{0:T(512)(128)(2,1)S(1)} all-reduce(bf16[512]{0:T(512)(128)(2,1)S(1)} %fusion.39), channel_id=1, replica_groups=mesh['ra'=16,'cb'=8] {'ra'}, use_global_device_ids=true, to_apply=%region_2.0 | all-reduce | flops 512 | bytes 2048 | tf_op jit(solution)/shard_map/psum | solution.py:65
  49.7 0.0 copy-done.11
  49.7 0.0 copy-done.12
  49.7 0.1 slice_reduce_fusion.3
  49.8 0.0 copy-done.13
  49.8 0.0 copy-done.14
  49.8 0.6 slice_reduce_fusion.4
  50.4 0.0 copy-done.8
  50.4 0.0 copy-done.9
  50.4 0.7 slice_reduce_fusion.2
  51.2 54.9 %all-reduce.11.cloned.1.call-done = (bf16[512,1056]{0,1:T(8,128)(2,1)}, bf16[512,1056]{0,1:T(8,128)(2,1)}) async-done(((bf16[512,1056]{0,1:T(8,128)(2,1)}, bf16[512,1056]{0,1:T(8,128)(2,1)}), (bf16[512,1056]{0,1:T(8,128)(2,1)}, bf16[512,1056]{0,1:T(8,128)(2,1)})) %all-reduce.11.cloned.1.call-update) | async-done | bytes 2162704 | tf_op jit(solution)/shard_map/psum | solution.py:67
  106.0 3.4 %multiply_multiply_fusion.3 = (f32[512,1056]{0,1:T(8,128)}, f32[512,1056]{0,1:T(8,128)S(1)}) fusion(bf16[512,1056]{0,1:T(8,128)(2,1)} %get-tuple-element.28, f32[1056]{0:T(1024)S(1)} %get-tuple-element.39, f32[512]{0:T(512)S(1)} %add_rsqrt_fusion.1, f32[1056]{0:T(1024)S(1)} %get-tuple-element.24, bf16[512,1056]{0,1:T(8,128)(2,1)} %get-tuple-element.27), kind=kLoop, calls=%fused_computation.41 | loop fusion | flops 3244032 | bytes 6498560 | tf_op jit(solution)/shard_map/mul | solution.py:71
  109.4 3.0 %copy.21 = f32[512,1056]{1,0:T(8,128)} copy(f32[512,1056]{0,1:T(8,128)} %get-tuple-element.37) | data formatting | bytes 4325376 | tf_op jit(solution)/shard_map/mul | solution.py:71
  112.4 1.9 copy.22
  114.4 7.5 %fusion.30 = bf16[512,192]{0,1:T(8,128)(2,1)S(1)} fusion(f32[64,8,1056]{2,1,0:T(8,128)} %bitcast.39, f32[1056]{0:T(1024)S(1)} %get-tuple-element.12, f32[1056]{0:T(1024)S(1)} %get-tuple-element.13, f32[1056]{0:T(1024)S(1)} %get-tuple-element.14, f32[1056]{0:T(1024)S(1)} %get-tuple-element.22, f32[64,8,1056]{2,1,0:T(8,128)} %bitcast.38, ...), kind=kOutput, calls=%fused_computation.46 | convolution fusion | flops 217448448 | bytes 5391360 | tf_op jit(solution)/shard_map/dot_general | solution.py:81
  121.9 1.3 broadcast_in_dim.8
  123.2 6.4 %all-to-all-start = ((bf16[8,512,192]{1,2,0:T(8,128)(2,1)}), bf16[8,512,192]{1,2,0:T(8,128)(2,1)S(1)}, u32[]{:S(2)}, u32[]{:S(2)}) async-start(bf16[8,512,192]{1,2,0:T(8,128)(2,1)} %broadcast_in_dim.8), calls=%async_computation | async-start | bytes 3145728 | tf_op jit(solution)/shard_map/all_to_all | solution.py:18
  129.6 0.0 all-reduce.9.cloned.1.call-start
  129.6 1.3 fusion.53
  130.9 19.3 %all-to-all-done = bf16[8,512,192]{1,2,0:T(8,128)(2,1)S(1)} async-done(((bf16[8,512,192]{1,2,0:T(8,128)(2,1)}), bf16[8,512,192]{1,2,0:T(8,128)(2,1)S(1)}, u32[]{:S(2)}, u32[]{:S(2)}) %all-to-all-start) | async-done | bytes 1572896 | tf_op jit(solution)/shard_map/all_to_all | solution.py:18
  150.2 0.2 convert_reduce_fusion.1
  150.4 0.8 fusion.43
  151.2 0.0 copy-start.3
  151.3 0.0 copy-done.1
  151.3 0.0 copy-done.10
  151.3 1.6 convolution_convert_fusion.1
  152.9 0.0 copy-done.3
  152.9 1.6 convolution_convert_fusion
  154.5 0.0 all-reduce.9.cloned.1.call-update
  154.5 31.2 %psum.46 = bf16[512]{0:T(512)(128)(2,1)S(1)} all-reduce(bf16[512]{0:T(512)(128)(2,1)S(1)} %get-tuple-element.29), channel_id=1, replica_groups=mesh['ra'=16,'cb'=8] {'ra'}, use_global_device_ids=true, to_apply=%region_7.8 | all-reduce | flops 512 | bytes 2048 | tf_op jit(solution)/shard_map/psum | solution.py:65
  185.7 56.5 %all-reduce.9.cloned.1.call-done = (bf16[512,1056]{0,1:T(8,128)(2,1)}, bf16[512,1056]{0,1:T(8,128)(2,1)}) async-done(((bf16[512,1056]{0,1:T(8,128)(2,1)}, bf16[512,1056]{0,1:T(8,128)(2,1)}), (bf16[512,1056]{0,1:T(8,128)(2,1)}, bf16[512,1056]{0,1:T(8,128)(2,1)})) %all-reduce.9.cloned.1.call-update) | async-done | bytes 2162704 | tf_op jit(solution)/shard_map/psum | solution.py:67
  242.2 3.4 %multiply_multiply_fusion.1 = (f32[512,1056]{0,1:T(8,128)}, f32[512,1056]{0,1:T(8,128)S(1)}) fusion(bf16[512,1056]{0,1:T(8,128)(2,1)} %get-tuple-element.26, f32[1056]{0:T(1024)S(1)} %get-tuple-element.40, f32[512]{0:T(512)S(1)} %add_rsqrt_fusion, f32[1056]{0:T(1024)S(1)} %get-tuple-element.23, bf16[512,1056]{0,1:T(8,128)(2,1)} %get-tuple-element.25), kind=kLoop, calls=%fused_computation.39 | loop fusion | flops 3244032 | bytes 6498560 | tf_op jit(solution)/shard_map/mul | solution.py:71
  245.6 3.0 %copy.23 = f32[512,1056]{1,0:T(8,128)} copy(f32[512,1056]{0,1:T(8,128)} %get-tuple-element.33) | data formatting | bytes 4325376 | tf_op jit(solution)/shard_map/mul | solution.py:71
  248.7 0.0 copy-start.18
  248.7 0.0 copy-start.19
  248.7 0.0 copy-start.20
  248.7 0.0 copy-start.21
  248.7 0.0 copy-start.22
  248.7 1.9 copy.24
  250.7 0.0 copy-done.7
  250.7 0.0 copy-done.15
  250.7 0.0 copy-done.16
  250.7 7.4 %fusion.33 = bf16[512,192]{0,1:T(8,128)(2,1)S(1)} fusion(f32[64,8,1056]{2,1,0:T(8,128)} %bitcast.37, f32[1056]{0:T(1024)S(1)} %copy-done.18, f32[1056]{0:T(1024)S(1)} %copy-done.19, f32[1056]{0:T(1024)S(1)} %copy-done.17, f32[1056]{0:T(1024)S(1)} %copy-done.15, f32[64,8,1056]{2,1,0:T(8,128)} %bitcast.36, f32[1056]{0:T(1024)S(1)} %copy-done.21, ...), kind=kOutput, calls=%fused_computation.47 | convolution fusion | flops 217448448 | bytes 5029888 | tf_op jit(solution)/shard_map/dot_general | solution.py:81
  258.2 0.1 broadcast_in_dim.9
  258.3 0.0 copy-start.4
  258.3 26.8 %all_to_all.10 = bf16[8,512,192]{1,2,0:T(8,128)(2,1)S(1)} all-to-all(bf16[8,512,192]{1,2,0:T(8,128)(2,1)S(1)} %broadcast_in_dim.9), channel_id=1, replica_groups=mesh['ra'=16,'cb'=8] {'cb'}, dimensions={0} | all-to-all | bytes 3145728 | tf_op jit(solution)/shard_map/all_to_all | solution.py:18
  285.1 0.2 convert_reduce_fusion
  285.3 0.8 fusion.41
  (24 shorter events, 0.1 us)
Async XLA Ops:
  6.5 3.0 %copy-start.5 = (f32[2,192,1056]{2,1,0:T(8,128)S(1)}, f32[2,192,1056]{2,1,0:T(8,128)}, u32[]{:S(2)}) copy-start(f32[2,192,1056]{2,1,0:T(8,128)} %param.14) | copy-start | bytes 4866052
  6.5 99.5 %all-reduce.11.cloned.1.call-start = ((), (), s32[]{:S(2)}) async-start(), calls=%async_computation.3 | async-start | bytes 4325376 | tf_op jit(solution)/shard_map/psum | solution.py:67
  7.9 1.7 copy-start.2
  9.7 1.6 copy-start
  11.3 1.7 copy-start.6
  12.9 36.8 %copy-start.11 = (f32[2,1056]{1,0:T(2,128)S(1)}, f32[2,1056]{1,0:T(2,128)}, u32[]{:S(2)}) copy-start(f32[2,1056]{1,0:T(2,128)} %param.17) | copy-start | bytes 25348
  12.9 36.8 %copy-start.12 = (f32[2,1056]{1,0:T(2,128)S(1)}, f32[2,1056]{1,0:T(2,128)}, u32[]{:S(2)}) copy-start(f32[2,1056]{1,0:T(2,128)} %param.15) | copy-start | bytes 25348
  12.9 36.9 %copy-start.13 = (f32[2,1056]{1,0:T(2,128)S(1)}, f32[2,1056]{1,0:T(2,128)}, u32[]{:S(2)}) copy-start(f32[2,1056]{1,0:T(2,128)} %param.21) | copy-start | bytes 25348
  12.9 36.9 %copy-start.14 = (f32[2,1056]{1,0:T(2,128)S(1)}, f32[2,1056]{1,0:T(2,128)}, u32[]{:S(2)}) copy-start(f32[2,1056]{1,0:T(2,128)} %param.20) | copy-start | bytes 25348
  12.9 37.5 %copy-start.8 = (f32[2,3,1056]{2,0,1:T(2,128)S(1)}, f32[2,3,1056]{2,0,1:T(2,128)}, u32[]{:S(2)}) copy-start(f32[2,3,1056]{2,0,1:T(2,128)} %param.19) | copy-start | bytes 76036
  12.9 37.5 %copy-start.9 = (f32[2,3,1056]{2,0,1:T(2,128)S(1)}, f32[2,3,1056]{2,0,1:T(2,128)}, u32[]{:S(2)}) copy-start(f32[2,3,1056]{2,0,1:T(2,128)} %param.18) | copy-start | bytes 76036
  123.2 28.1 %copy-start.1 = (bf16[2,192,1056]{2,1,0:T(8,128)(2,1)S(1)}, bf16[2,192,1056]{2,1,0:T(8,128)(2,1)}, u32[]{:S(2)}) copy-start(bf16[2,192,1056]{2,1,0:T(8,128)(2,1)} %copy-done) | copy-start | bytes 2433028
  123.2 27.0 %all-to-all-start = ((bf16[8,512,192]{1,2,0:T(8,128)(2,1)}), bf16[8,512,192]{1,2,0:T(8,128)(2,1)S(1)}, u32[]{:S(2)}, u32[]{:S(2)}) async-start(bf16[8,512,192]{1,2,0:T(8,128)(2,1)} %broadcast_in_dim.8), calls=%async_computation | async-start | bytes 3145728 | tf_op jit(solution)/shard_map/all_to_all | solution.py:18
  129.6 112.6 %all-reduce.9.cloned.1.call-start = ((), (), s32[]{:S(2)}) async-start(), calls=%async_computation.2 | async-start | bytes 4325376 | tf_op jit(solution)/shard_map/psum | solution.py:67
  150.2 1.1 copy-start.10
  151.2 1.6 copy-start.3
  248.7 2.0 copy-start.7
  248.7 2.0 copy-start.15
  248.7 2.0 copy-start.16
  248.7 2.0 copy-start.17
  248.7 2.0 copy-start.18
  248.7 2.0 copy-start.19
  248.7 2.0 copy-start.20
  248.7 2.0 copy-start.21
  248.7 2.0 copy-start.22
  258.3 27.0 %copy-start.4 = (bf16[512,192]{0,1:T(8,128)(2,1)S(1)}, bf16[512,192]{0,1:T(8,128)(2,1)}, u32[]{:S(2)}) copy-start(bf16[512,192]{0,1:T(8,128)(2,1)} %copy-done.3) | copy-start | bytes 589828
  258.3 27.0 %copy-start.23 = (f32[1,192]{1,0:T(1,128)S(1)}, f32[1,192]{1,0:T(1,128)}, u32[]{:S(2)}) copy-start(f32[1,192]{1,0:T(1,128)} %get-tuple-element.31) | copy-start | bytes 2308
Sparse Core Ops, SparseCore 0:
  13.1 92.9 all-reduce.10
  154.6 87.5 all-reduce.8
where the time goes:
time: 293 us
  waiting for transfers between devices  131 us (45%)
  blocking collectives  93.7 us (32%)
  matrix products  21.4 us (7%)
  local copies, waits for them, and re-layouts  15.6 us (5%)
  between operations  13.7 us (5%)
  other arithmetic  11.6 us (4%)
  starting transfers between devices  6.42 us (2%)
    psum x2, waiting for transfers between devices, shards(): lax.psum(value_part.astype(jnp.bfloat16), 'ra').astype(jnp.float32)  111 us
    psum x2, blocking collectives, shards(): lax.psum(local_squares.astype(jnp.bfloat16), 'ra').astype(jnp.float32)  66.9 us
    all_to_all x1, blocking collectives, copy_for_each(): return lax.all_to_all(copies, axis, split_axis=0, concat_axis=0, tiled=True)  26.8 us
    all_to_all x1, waiting for transfers between devices, copy_for_each(): return lax.all_to_all(copies, axis, split_axis=0, concat_axis=0, tiled=True)  19.3 us
    dot_general x2, matrix products, shards(): jnp.dot(hidden, down_weight[depth_index].astype(jnp.bfloat16), preferred_...  15 us
    mul x2, other arithmetic, shards(): gate_pre * inverse_rms * gate_scale[depth_index]  6.76 us
    all_to_all x1, starting transfers between devices, copy_for_each(): return lax.all_to_all(copies, axis, split_axis=0, concat_axis=0, tiled=True)  6.42 us
    mul x2, local copies, waits for them, and re-layouts, shards(): gate_pre * inverse_rms * gate_scale[depth_index]  6.08 us
  transfers between devices with their start and end apart: 3, of which 3 were waited for; matrix products, arithmetic and copies ran while one was open for 1% of the time, Pallas kernels for 0%

commit v1 on v0

v1 whole, which is shorter than its diff:
```python
import functools

import jax
import jax.numpy as jnp
from jax import lax
from jax.experimental import pallas as pl
from jax.experimental.pallas import tpu as pltpu
from jax.sharding import PartitionSpec as P

D = 3072
TAPS = 3
LAYERS = 2
SEQ_LEN = 8
epsilon = 1e-06
residual_keep = 0.5

MESH = pl.DeviceIdType.MESH
F32 = jnp.float32
BF16 = jnp.bfloat16

TOK = 256
ROWS = 16
W = 192
FFD = 1056
MAIN = 512
LEFT = FFD - 2 * MAIN
PRE = (2 * MAIN + 128, 2 * MAIN, 2 * MAIN + 128, 2 * MAIN)
HID = (MAIN + 128, MAIN, MAIN + 128, MAIN)
ORDER = ((0, 1, 2, 3), (1, 0, 3, 2), (2, 3, 0, 1), (3, 2, 1, 0))
CH = range(4)


def pick(axis, index, rank):
    return tuple(index if i == axis else slice(None) for i in range(rank))


def kernel(
    tokens,
    norm_gain,
    gate_weight,
    gate_scale,
    value_weight,
    value_scale,
    gate_conv,
    value_conv,
    gate_bias,
    value_bias,
    down_weight,
    down_scale,
    out,
    *scratch,
):
    it = iter(scratch)
    take = lambda n: [next(it) for _ in range(n)]
    (stream, squares, normed, gain, dscale) = take(5)
    (wide, dwide) = take(2)
    wcols = take(2)
    drows = take(2)
    params = take(6)
    snd = [take(4) for _ in range(4)]
    kept = [take(4) for _ in range(4)]
    got = [take(4) for _ in range(4)]
    hid = take(4)
    (total, ysend, yrecv) = take(3)
    (load_sem, peer_send, peer_recv, rs_send, rs_recv, ag_send, ag_recv, y_send, y_recv, out_sem) = take(10)

    ra = lax.axis_index("ra")
    cb = lax.axis_index("cb")
    x, z = ra % 4, ra // 4
    y, c = cb // 2, cb % 2

    def at(nx, nz):
        return nz * 4 + nx

    def flip(v):
        return v + 1 - 2 * (v % 2)

    def choose(first, second):
        return first * (1 - c) + second * c

    xa, xb, za, zb = at(flip(x), z), at(3 - x, z), at(x, flip(z)), at(x, 3 - z)
    bxa, bxb, bza, bzb = ((x + 1) // 2) % 2, x // 2, ((z + 1) // 2) % 2, z // 2
    mates = (choose(xa, zb), choose(xb, za), choose(za, xb), choose(zb, xa))
    bits = (choose(bxa, bzb), choose(bxb, bza), choose(bza, bxb), choose(bzb, bxa))
    peer = (ra, y * 2 + 1 - c)
    ymates = ((ra, flip(y) * 2 + c), (ra, (3 - y) * 2 + c))

    sources = (gate_scale, value_scale, gate_conv, value_conv, gate_bias, value_bias)
    loads = {}

    def load(name, src, dst, index):
        loads[name] = pltpu.make_async_copy(src, dst, load_sem.at[index])
        loads[name].start()

    load("x", tokens.at[pl.ds(c * 16, 16)], stream, 0)
    load("gain", norm_gain, gain, 1)
    for layer in range(LAYERS):
        load(("g", layer), gate_weight.at[layer], wide.at[layer, 0], 2 + layer * 3)
        load(("v", layer), value_weight.at[layer], wide.at[layer, 1], 3 + layer * 3)
        load(("d", layer), down_weight.at[layer], dwide.at[layer], 4 + layer * 3)
        if layer == 0:
            load("ds", down_scale, dscale, 8)
            for i, src in enumerate(sources):
                load(("p", i), src, params[i].at[0], 9 + i)

    barrier = pltpu.get_barrier_semaphore()
    for mate in mates:
        pl.semaphore_signal(barrier, inc=1, device_id=(mate, cb), device_id_type=MESH)
    for target in (peer, *ymates):
        pl.semaphore_signal(barrier, inc=1, device_id=target, device_id_type=MESH)

    sent = []

    def remote(src, dst, send_sem, recv_sem, target):
        copy = pltpu.make_async_remote_copy(
            src_ref=src, dst_ref=dst, send_sem=send_sem, recv_sem=recv_sem,
            device_id=target, device_id_type=MESH,
        )
        copy.start()
        sent.append(copy)
        return copy

    line = lax.broadcasted_iota(jnp.int32, (LEFT, 128), 1)
    row = lax.broadcasted_iota(jnp.int32, (LEFT, 128), 0)
    put_gate = (line == row).astype(F32).astype(BF16)
    put_value = (line == row + LEFT).astype(F32).astype(BF16)

    def cast_up(layer):
        loads[("g", layer)].wait()
        loads[("v", layer)].wait()
        g, v = wide.at[layer, 0], wide.at[layer, 1]
        wcols[0][layer, 0, :, 0:MAIN] = g[:, 0:MAIN].astype(BF16)
        wcols[0][layer, 0, :, MAIN : 2 * MAIN] = v[:, 0:MAIN].astype(BF16)
        low = jnp.dot(g[:, 2 * MAIN : FFD].astype(BF16), put_gate, preferred_element_type=F32)
        low += jnp.dot(v[:, 2 * MAIN : FFD].astype(BF16), put_value, preferred_element_type=F32)
        wcols[0][layer, 0, :, 2 * MAIN : 2 * MAIN + 128] = low.astype(BF16)
        wcols[1][layer, 0, :, 0:MAIN] = g[:, MAIN : 2 * MAIN].astype(BF16)
        wcols[1][layer, 0, :, MAIN : 2 * MAIN] = v[:, MAIN : 2 * MAIN].astype(BF16)

    def cast_down(layer):
        loads[("d", layer)].wait()
        d = dwide.at[layer]
        drows[0][layer, 0, 0:MAIN, :] = d[0:MAIN, :].astype(BF16)
        drows[0][layer, 0, MAIN : MAIN + LEFT, :] = d[2 * MAIN : FFD, :].astype(BF16)
        drows[0][layer, 0, MAIN + LEFT : MAIN + 128, :] = jnp.zeros((128 - LEFT, W), BF16)
        drows[1][layer, 0, :, :] = d[MAIN : 2 * MAIN, :].astype(BF16)

    from_peer = {}

    def give(name, ref_from, ref_to, index):
        from_peer[name] = remote(ref_from, ref_to, peer_send.at[index], peer_recv.at[index], peer)

    def need(name):
        if name in from_peer:
            from_peer.pop(name).wait_recv()

    lane = lax.broadcasted_iota(jnp.int32, (TOK, 128), 1)

    def prepare(layer):
        wideal = stream[...].reshape(TOK, W).astype(F32)
        own = jnp.sum(wideal * wideal, axis=1, keepdims=True)
        squares[...] = jnp.where(lane == 2 * LEFT, own, 0.0).reshape(squares.shape)
        normed[...] = (wideal * gain[layer : layer + 1, :]).astype(BF16).reshape(normed.shape)

    def project(layer, k, index):
        rows = normed[index].reshape(TOK // 2, W)
        product = jnp.dot(rows, wcols[k % 2][layer, k // 2], preferred_element_type=F32)
        if k == 0:
            tail = product[:, 2 * MAIN :] + squares[index].reshape(TOK // 2, 128)
            return product[:, : 2 * MAIN], tail
        return product, None

    def store(ref, value):
        main, tail = value
        lead = ref.shape[:-1]
        if tail is None:
            ref[...] = main.astype(BF16).reshape(ref.shape)
        else:
            ref[..., 0 : 2 * MAIN] = main.astype(BF16).reshape(*lead, 2 * MAIN)
            ref[..., 2 * MAIN :] = tail.astype(BF16).reshape(*lead, 128)

    def rs_copy(layer, step, k):
        dim = ORDER[k][step]
        return remote(
            snd[step][k].at[layer], got[step][k].at[layer],
            rs_send.at[layer, step, k], rs_recv.at[layer, step, k], (mates[dim], cb),
        )

    keep_row = lax.broadcasted_iota(jnp.int32, (ROWS, 1), 0) % SEQ_LEN

    def mix(pre, taps, bias):
        back_one = jnp.where(keep_row >= 1, pltpu.roll(pre, 1, 0), 0.0)
        back_two = jnp.where(keep_row >= 2, pltpu.roll(pre, 2, 0), 0.0)
        return bias + back_two * taps[0] + back_one * taps[1] + pre * taps[2]

    def gated(layer, slot, cols, gate_sum, value_sum, inverse):
        scale_g, scale_v, conv_g, conv_v, bias_g, bias_v = params
        one = lambda ref: ref[slot, layer : layer + 1, cols]
        taps = lambda ref: [ref[slot, layer, i : i + 1, cols] for i in range(TAPS)]
        gate = mix(gate_sum * inverse * one(scale_g), taps(conv_g), one(bias_g))
        value = mix(value_sum * inverse * one(scale_v), taps(conv_v), one(bias_v))
        return (gate / (1.0 + jnp.exp(-gate)) * value).astype(BF16)

    loads["x"].wait()
    loads["gain"].wait()
    for layer in range(LAYERS):
        prepare(layer)
        if layer == 0:
            cast_up(0)
            pl.semaphore_wait(barrier, 7)
            for i in range(2):
                give(("w", i, 0), wcols[i].at[0, 0], wcols[i].at[0, 1], i)
        flights = {}
        for k in CH:
            if k >= 2:
                need(("w", k - 2, layer))
            dim = ORDER[k][0]
            store(snd[0][k].at[layer], project(layer, k, pick(dim, 1 - bits[dim], 4)))
            flights[k] = rs_copy(layer, 0, k)
        for k in CH:
            dim = ORDER[k][0]
            store(kept[0][k].at[layer], project(layer, k, pick(dim, bits[dim], 4)))
        if layer == 0:
            cast_down(0)
            for i in range(2):
                give(("d", i, 0), drows[i].at[0, 0], drows[i].at[0, 1], 4 + i)
            loads["ds"].wait()
            for i in range(6):
                loads[("p", i)].wait()
                give(("p", i), params[i].at[0], params[i].at[1], 8 + i)
            cast_up(1)
            for i in range(2):
                give(("w", i, 1), wcols[i].at[1, 0], wcols[i].at[1, 1], 2 + i)
            cast_down(1)
            for i in range(2):
                give(("d", i, 1), drows[i].at[1, 0], drows[i].at[1, 1], 6 + i)
        for step in range(1, 4):
            for k in CH:
                left = sorted(ORDER[k][step - 1 :])
                left.remove(ORDER[k][step - 1])
                dim = ORDER[k][step]
                axis = left.index(dim)
                rank = len(left)
                flights[k].wait_recv()
                away, home = pick(axis, 1 - bits[dim], rank), pick(axis, bits[dim], rank)
                before, arrived = kept[step - 1][k].at[layer], got[step - 1][k].at[layer]
                snd[step][k][layer] = before[away] + arrived[away]
                flights[k] = rs_copy(layer, step, k)
                kept[step][k][layer] = before[home] + arrived[home]
        if layer == 0:
            for i in range(6):
                need(("p", i))
        inverse = None
        for k in CH:
            slot, part = k // 2, k % 2
            flights[k].wait_recv()
            final = kept[3][k][layer].astype(F32) + got[3][k][layer].astype(F32)
            if k == 0:
                low = final[:, 2 * MAIN :]
                own_lane = lax.broadcasted_iota(jnp.int32, (ROWS, 128), 1) == 2 * LEFT
                mean = jnp.sum(jnp.where(own_lane, low, 0.0), axis=1, keepdims=True) / D
                inverse = lax.rsqrt(mean + epsilon)
            mine = tuple(bits)
            cols = slice(part * MAIN, (part + 1) * MAIN)
            hid[k][(layer, *mine, slice(None), slice(0, MAIN))] = gated(
                layer, slot, cols, final[:, 0:MAIN], final[:, MAIN : 2 * MAIN], inverse
            )
            if part == 0:
                low = final[:, 2 * MAIN :]
                high = pltpu.roll(low, 128 - LEFT, 1)
                hid[k][(layer, *mine, slice(None), slice(MAIN, MAIN + 128))] = jnp.zeros((ROWS, 128), BF16)
                hid[k][(layer, *mine, slice(None), slice(MAIN, MAIN + LEFT))] = gated(
                    layer, slot, slice(2 * MAIN, FFD), low[:, 0:LEFT], high[:, 0:LEFT], inverse
                )
            flights[k] = gather(layer, 3, k, hid, bits, mates, cb, ag_send, ag_recv, remote)
        for step in (2, 1, 0):
            for k in CH:
                flights[k].wait_recv()
                flights[k] = gather(layer, step, k, hid, bits, mates, cb, ag_send, ag_recv, remote)
        for k in CH:
            if k >= 2:
                need(("d", k - 2, layer))
            flights[k].wait_recv()
            part = jnp.dot(
                hid[k][layer].reshape(TOK, HID[k]), drows[k % 2][layer, k // 2], preferred_element_type=F32
            )
            if k == 0:
                total[...] = part
            elif k < 3:
                total[...] += part
            else:
                ysend[layer, 0] = (total[...] + part).astype(BF16).reshape(2, TOK // 2, W)
        hops = [
            remote(
                ysend.at[layer, 0, half], yrecv.at[layer, 0, half],
                y_send.at[layer, 0, half], y_recv.at[layer, 0, half], ymates[half],
            )
            for half in range(2)
        ]
        for half in range(2):
            hops[half].wait_recv()
            ysend[layer, 1, half] = ysend[layer, 0, half] + yrecv[layer, 0, half]
            hops[half] = remote(
                ysend.at[layer, 1, half], yrecv.at[layer, 1, half],
                y_send.at[layer, 1, half], y_recv.at[layer, 1, half], ymates[1 - half],
            )
        for half in range(2):
            hops[half].wait_recv()
            rows = slice(half * 8, half * 8 + 8)
            branch = (ysend[layer, 1, half].astype(F32) + yrecv[layer, 1, half].astype(F32)) * dscale[layer : layer + 1, :]
            old = stream[rows].reshape(TOK // 2, W).astype(F32)
            stream[rows] = (residual_keep * old + branch).astype(BF16).reshape(8, ROWS, W)
    here = pl.ds(c * 16, 16)
    mine = pltpu.make_async_copy(stream, out.at[here], out_sem.at[0])
    mine.start()
    last = remote(stream, out.at[here], out_sem.at[1], out_sem.at[2], peer)
    mine.wait()
    last.wait_recv()
    for copy in sent:
        copy.wait_send()


def gather(layer, step, k, hid, bits, mates, cb, ag_send, ag_recv, remote):
    fixed = ORDER[k][: step + 1]
    index = (layer, *(bits[i] if i in fixed else slice(None) for i in range(4)))
    return remote(
        hid[k].at[index], hid[k].at[index],
        ag_send.at[layer, step, k], ag_recv.at[layer, step, k], (mates[ORDER[k][step]], cb),
    )


def shards(tokens, *rest):
    vm = pltpu.VMEM
    dma = pltpu.SemaphoreType.DMA
    scratch = [
        vm((16, ROWS, W), BF16),
        vm((2, 2, 2, 2, ROWS, 128), F32),
        vm((2, 2, 2, 2, ROWS, W), BF16),
        vm((LAYERS, W), F32),
        vm((LAYERS, W), F32),
        vm((LAYERS, 2, W, FFD), F32),
        vm((LAYERS, FFD, W), F32),
        *(vm((LAYERS, 2, W, PRE[i]), BF16) for i in range(2)),
        *(vm((LAYERS, 2, HID[i], W), BF16) for i in range(2)),
        *(vm((2, LAYERS, FFD), F32) for _ in range(2)),
        *(vm((2, LAYERS, TAPS, FFD), F32) for _ in range(2)),
        *(vm((2, LAYERS, FFD), F32) for _ in range(2)),
    ]
    for _ in range(3):
        for step in range(4):
            for k in CH:
                scratch.append(vm((LAYERS, *(2,) * (3 - step), ROWS, PRE[k]), BF16))
    scratch += [vm((LAYERS, 2, 2, 2, 2, ROWS, HID[k]), BF16) for k in CH]
    scratch += [vm((TOK, W), F32), vm((LAYERS, 2, 2, TOK // 2, W), BF16), vm((LAYERS, 2, 2, TOK // 2, W), BF16)]
    scratch += [
        dma((16,)), dma((16,)), dma((16,)),
        dma((LAYERS, 4, 4)), dma((LAYERS, 4, 4)), dma((LAYERS, 4, 4)), dma((LAYERS, 4, 4)),
        dma((LAYERS, 2, 2)), dma((LAYERS, 2, 2)), dma((3,)),
    ]
    count = tokens.shape[0]
    result = pl.pallas_call(
        kernel,
        out_shape=jax.ShapeDtypeStruct((count // ROWS, ROWS, W), BF16),
        in_specs=[pl.BlockSpec(memory_space=pl.ANY)] * 12,
        out_specs=pl.BlockSpec(memory_space=pl.ANY),
        scratch_shapes=scratch,
        compiler_params=pltpu.CompilerParams(
            collective_id=0, has_side_effects=True, vmem_limit_bytes=60 * 1024 * 1024
        ),
        name="two_layers",
    )(tokens.reshape(count // ROWS, ROWS, W), *rest)
    return result.reshape(count, W)


def solution(mesh):
    placed = (
        P(None, "ra"),
        P(None, "ra"),
        P(None, "ra", "cb"),
        P(None, "cb"),
        P(None, "ra", "cb"),
        P(None, "cb"),
        P(None, None, "cb"),
        P(None, None, "cb"),
        P(None, "cb"),
        P(None, "cb"),
        P(None, "cb", "ra"),
        P(None, "ra"),
    )
    return jax.shard_map(
        shards, mesh=mesh, in_specs=placed, out_specs=P(None, "ra"), check_vma=False
    )
```

time: 293 us -> 106 us (0.36)
  waiting for transfers between devices: 131 us -> 0 us
  Pallas kernels: 0 us -> 97 us
  blocking collectives: 93.7 us -> 0 us
  matrix products: 21.4 us -> 0 us
  between operations: 13.7 us -> 0.01 us
  other arithmetic: 11.6 us -> 0 us
  local copies, waits for them, and re-layouts: 15.6 us -> 9.16 us
  starting transfers between devices: 6.42 us -> 0 us
    psum x2 -> x0, waiting for transfers between devices: 111 us -> none  [shards(): lax.psum(value_part.astype(jnp.bfloat16), 'ra').astype(jnp.float32)]
    pallas_call x0 -> x1, Pallas kernels: none -> 97 us  [shards(): pl.pallas_call(kernel, out_shape=jax.ShapeDtypeStruct((count // ROWS, ROW...]
    psum x2 -> x0, blocking collectives: 66.9 us -> none  [shards(): lax.psum(local_squares.astype(jnp.bfloat16), 'ra').astype(jnp.float32)]
    all_to_all x1 -> x0, blocking collectives: 26.8 us -> none  [copy_for_each(): return lax.all_to_all(copies, axis, split_axis=0, concat_axis=0, tiled=True)]
    dot_general x6 -> x0, matrix products: 21.4 us -> none  [the longest x2 15 us: shards(): jnp.dot(hidden, down_weight[depth_index].astype(jnp.bfloat16), preferred_...]
    all_to_all x1 -> x0, waiting for transfers between devices: 19.3 us -> none  [copy_for_each(): return lax.all_to_all(copies, axis, split_axis=0, concat_axis=0, tiled=True)]
    mul x4 -> x0, local copies, waits for them, and re-layouts: 9.92 us -> none  [the longest x2 6.08 us: shards(): gate_pre * inverse_rms * gate_scale[depth_index]]
    unnamed x48 -> x4, local copies, waits for them, and re-layouts: 0.1 us -> 7.41 us
  transfers between devices with their start and end apart: 3 -> 0, of which waited for: 3 -> 0; matrix products, arithmetic and copies ran while one was open for 1% -> 0% of each run, Pallas kernels for 0% -> 0%
where the time goes in v1:
time: 106 us
  Pallas kernels  97 us (92%)
  local copies, waits for them, and re-layouts  9.16 us (9%)
    pallas_call x1, Pallas kernels, shards(): pl.pallas_call(kernel, out_shape=jax.ShapeDtypeStruct((count // ROWS, ROW...  97 us
    unnamed x4, local copies, waits for them, and re-layouts  7.41 us

profile of v1, /device:TPU:1, one launch (start us, length us, event | category | flops | bytes accessed | tf_op | source)
XLA Modules:
  0.0 106.1 jit_solution(10319313666757193130)
XLA Ops:
  0.0 1.4 %copy.14.gate_conv = f32[2,3,1056]{2,1,0:T(4,128)} copy(f32[2,3,1056]{2,0,1:T(2,128)} %param.18) | data formatting | bytes 50688 | tf_op args[6]
  1.4 1.4 %copy.15.value_conv = f32[2,3,1056]{2,1,0:T(4,128)} copy(f32[2,3,1056]{2,0,1:T(2,128)} %param.19) | data formatting | bytes 50688 | tf_op args[7]
  2.7 1.8 %copy.13 = bf16[512,192]{1,0:T(8,128)(2,1)} copy(bf16[512,192]{0,1:T(8,128)(2,1)} %param.12) | data formatting | bytes 393216 | tf_op args[0]
  4.5 2.9 %copy.16.down_weight = f32[2,1056,192]{2,1,0:T(8,128)} copy(f32[2,1056,192]{1,2,0:T(8,128)} %param.22) | data formatting | bytes 3244032 | tf_op args[10]
  7.4 97.0 %two_layers.1 = bf16[32,16,192]{2,1,0:T(8,128)(2,1)} custom-call(bf16[32,16,192]{2,1,0:T(8,128)(2,1)} %bitcast.3, f32[2,192]{1,0:T(2,128)} %norm_gain.1, f32[2,192,1056]{2,1,0:T(8,128)} %gate_weight.1, f32[2,1056]{1,0:T(2,128)} %gate_scale.1, f32[2,192,1056]{2,1,0:T(8,128)} %value_weight.1, f32[2,1056]{1,0:T(2,128)} %value_scale.1, ...), custom_call_target="tpu_custom_call" | custom-call | tf_op jit(solution)/shard_map/two_layers/pallas_call | solution.py:361
  104.4 1.8 %copy.17 = bf16[512,192]{0,1:T(8,128)(2,1)} copy(bf16[512,192]{1,0:T(8,128)(2,1)} %bitcast.2) | data formatting | bytes 393216 | tf_op jit(solution)/shard_map/reshape | solution.py:372

commit v2 on v1

v2 whole, which is shorter than its diff:
```python
import jax
import jax.numpy as jnp
from jax import lax
from jax.experimental import pallas as pl
from jax.experimental.pallas import tpu as pltpu
from jax.sharding import PartitionSpec as P

D = 3072
TAPS = 3
LAYERS = 2
SEQ_LEN = 8
epsilon = 1e-06
residual_keep = 0.5

MESH = pl.DeviceIdType.MESH
F32 = jnp.float32
BF16 = jnp.bfloat16

STREAMS = 2
TOK = 128
ROWS = 8
W = 192
FFD = 1056
MAIN = 512
LEFT = FFD - 2 * MAIN
PRE = (2 * MAIN + 128, 2 * MAIN, 2 * MAIN + 128, 2 * MAIN)
HID = (MAIN + 128, MAIN, MAIN + 128, MAIN)
ORDER = ((0, 1, 2, 3), (1, 0, 3, 2), (2, 3, 0, 1), (3, 2, 1, 0))
CH = range(4)
ST = range(STREAMS)


def pick(axis, index, rank):
    return tuple(index if i == axis else slice(None) for i in range(rank))


def kernel(
    tokens,
    norm_gain,
    gate_weight,
    gate_scale,
    value_weight,
    value_scale,
    gate_conv,
    value_conv,
    gate_bias,
    value_bias,
    down_weight,
    down_scale,
    out,
    *scratch,
):
    it = iter(scratch)
    take = lambda n: [next(it) for _ in range(n)]
    (stream, squares, normed, gain, dscale) = take(5)
    (wide, dwide) = take(2)
    wcols = take(2)
    drows = take(2)
    params = take(6)
    snd = [take(4) for _ in range(2)]
    kept = [take(4) for _ in range(2)]
    got = [take(4) for _ in range(2)]
    quad = take(4)
    pieces = take(4)
    hid = take(4)
    (total, ypart) = take(2)
    (load_sem, peer_send, peer_recv, rs_send, rs_recv, dx_send, dx_recv, ag_send, ag_recv, y_send, y_recv, out_sem) = take(12)

    ra = lax.axis_index("ra")
    cb = lax.axis_index("cb")
    x, z = ra % 4, ra // 4
    y, c = cb // 2, cb % 2

    def at(nx, nz):
        return nz * 4 + nx

    def flip(v):
        return v + 1 - 2 * (v % 2)

    def choose(first, second):
        return first * (1 - c) + second * c

    xa, xb, za, zb = at(flip(x), z), at(3 - x, z), at(x, flip(z)), at(x, 3 - z)
    xo, zo = at((x + 2) % 4, z), at(x, (z + 2) % 4)
    bxa, bxb, bza, bzb = ((x + 1) // 2) % 2, x // 2, ((z + 1) // 2) % 2, z // 2
    mates = (choose(xa, zb), choose(xb, za), choose(za, xb), choose(zb, xa))
    bits = (choose(bxa, bzb), choose(bxb, bza), choose(bza, bxb), choose(bzb, bxa))
    across = (choose(xo, zo), choose(zo, xo))
    peer = (ra, y * 2 + 1 - c)
    ymates = ((ra, flip(y) * 2 + c), (ra, (3 - y) * 2 + c), (ra, ((y + 2) % 4) * 2 + c))

    def ring(first, second):
        return (mates[first], cb), (mates[second], cb), (across[first // 2], cb)

    sources = (gate_scale, value_scale, gate_conv, value_conv, gate_bias, value_bias)
    loads = {}

    def load(name, src, dst, index):
        loads[name] = pltpu.make_async_copy(src, dst, load_sem.at[index])
        loads[name].start()

    for s in ST:
        load(("x", s), tokens.at[:, pl.ds(pl.multiple_of(c * 256 + s * TOK, TOK), TOK)], stream.at[s], s)
    load("gain", norm_gain, gain, 2)
    for layer in range(LAYERS):
        load(("g", layer), gate_weight.at[layer], wide.at[layer, 0], 3 + layer * 3)
        load(("v", layer), value_weight.at[layer], wide.at[layer, 1], 4 + layer * 3)
        load(("d", layer), down_weight.at[layer], dwide.at[layer], 5 + layer * 3)
        if layer == 0:
            load("ds", down_scale, dscale, 9)
            for i, src in enumerate(sources):
                load(("p", i), src, params[i].at[0], 10 + i)

    barrier = pltpu.get_barrier_semaphore()
    greet = [(m, cb) for m in (*mates, *across)] + [peer, *ymates]
    for target in greet:
        pl.semaphore_signal(barrier, inc=1, device_id=target, device_id_type=MESH)

    sent = []

    def remote(src, dst, send_sem, recv_sem, target):
        copy = pltpu.make_async_remote_copy(
            src_ref=src, dst_ref=dst, send_sem=send_sem, recv_sem=recv_sem,
            device_id=target, device_id_type=MESH,
        )
        copy.start()
        sent.append(copy)
        return copy

    line = lax.broadcasted_iota(jnp.int32, (LEFT, 128), 1)
    row = lax.broadcasted_iota(jnp.int32, (LEFT, 128), 0)
    put_gate = (line == row).astype(F32).astype(BF16)
    put_value = (line == row + LEFT).astype(F32).astype(BF16)

    def cast_up(layer):
        loads[("g", layer)].wait()
        loads[("v", layer)].wait()
        g, v = wide.at[layer, 0], wide.at[layer, 1]
        wcols[0][layer, 0, :, 0:MAIN] = g[:, 0:MAIN].astype(BF16)
        wcols[0][layer, 0, :, MAIN : 2 * MAIN] = v[:, 0:MAIN].astype(BF16)
        low = jnp.dot(g[:, 2 * MAIN : FFD].astype(BF16), put_gate, preferred_element_type=F32)
        low += jnp.dot(v[:, 2 * MAIN : FFD].astype(BF16), put_value, preferred_element_type=F32)
        wcols[0][layer, 0, :, 2 * MAIN : 2 * MAIN + 128] = low.astype(BF16)
        wcols[1][layer, 0, :, 0:MAIN] = g[:, MAIN : 2 * MAIN].astype(BF16)
        wcols[1][layer, 0, :, MAIN : 2 * MAIN] = v[:, MAIN : 2 * MAIN].astype(BF16)

    def cast_down(layer):
        loads[("d", layer)].wait()
        d = dwide.at[layer]
        drows[0][layer, 0, :, 0:MAIN] = d[:, 0:MAIN].astype(BF16)
        low = jnp.dot(d[:, 2 * MAIN : FFD].astype(BF16), put_gate, preferred_element_type=F32)
        drows[0][layer, 0, :, MAIN : MAIN + 128] = low.astype(BF16)
        drows[1][layer, 0, :, :] = d[:, MAIN : 2 * MAIN].astype(BF16)

    from_peer = {}

    def give(name, ref_from, ref_to, index):
        from_peer[name] = remote(ref_from, ref_to, peer_send.at[index], peer_recv.at[index], peer)

    def need(name):
        if name in from_peer:
            from_peer.pop(name).wait_recv()

    lane = lax.broadcasted_iota(jnp.int32, (TOK, 128), 1)

    def prepare(layer, s):
        values = jnp.transpose(stream[s].astype(F32))
        own = jnp.sum(values * values, axis=1, keepdims=True)
        squares[s] = jnp.where(lane == 2 * LEFT, own, 0.0).reshape(squares.shape[1:])
        rounded = (values * gain[layer : layer + 1, :]).astype(BF16).astype(F32)
        normed[s] = rounded.reshape(normed.shape[1:])

    def project(ref, layer, s, k, index):
        rows = normed[(s, *index)].reshape(TOK // 2, W).astype(BF16)
        product = jnp.dot(rows, wcols[k % 2][layer, k // 2], preferred_element_type=F32)
        if k == 0:
            tail = product[:, 2 * MAIN :] + squares[(s, *index)].reshape(TOK // 2, 128)
            ref[..., 2 * MAIN :] = tail.reshape(2, 2, 2, ROWS, 128).astype(BF16)
            ref[..., 0 : 2 * MAIN] = product[:, : 2 * MAIN].reshape(2, 2, 2, ROWS, 2 * MAIN).astype(BF16)
        else:
            ref[...] = product.reshape(2, 2, 2, ROWS, PRE[k]).astype(BF16)

    def halve(layer, s, step, k):
        return remote(
            snd[step][k].at[layer, s], got[step][k].at[layer, s],
            rs_send.at[layer, s, step, k], rs_recv.at[layer, s, step, k], (mates[ORDER[k][step]], cb),
        )

    keep_row = lax.broadcasted_iota(jnp.int32, (ROWS, 1), 0)

    def mix(pre, taps, bias):
        back_one = jnp.where(keep_row >= 1, pltpu.roll(pre, 1, 0), 0.0)
        back_two = jnp.where(keep_row >= 2, pltpu.roll(pre, 2, 0), 0.0)
        return bias + back_two * taps[0] + back_one * taps[1] + pre * taps[2]

    def gated(layer, slot, cols, gate_sum, value_sum, inverse):
        scale_g, scale_v, conv_g, conv_v, bias_g, bias_v = params
        one = lambda ref: ref[slot, layer : layer + 1, cols]
        taps = lambda ref: [ref[slot, i, layer : layer + 1, cols] for i in range(TAPS)]
        gate = mix(gate_sum * inverse * one(scale_g), taps(conv_g), one(bias_g))
        value = mix(value_sum * inverse * one(scale_v), taps(conv_v), one(bias_v))
        return (gate / (1.0 + jnp.exp(-gate)) * value).astype(BF16)

    flights = {}

    def first(layer, s, k):
        if k >= 2:
            need(("w", k - 2, layer))
        dim = ORDER[k][0]
        project(snd[0][k].at[layer, s], layer, s, k, pick(dim, 1 - bits[dim], 4))
        flights[s, k] = halve(layer, s, 0, k)

    def own_half(layer, s, k):
        dim = ORDER[k][0]
        project(kept[0][k].at[layer, s], layer, s, k, pick(dim, bits[dim], 4))

    def second(layer, s, k):
        left = sorted(ORDER[k][1:])
        dim = ORDER[k][1]
        axis = left.index(dim)
        flights[s, k].wait_recv()
        away, home = pick(axis, 1 - bits[dim], 3), pick(axis, bits[dim], 3)
        before, arrived = kept[0][k].at[layer, s], got[0][k].at[layer, s]
        snd[1][k][layer, s] = before[away] + arrived[away]
        flights[s, k] = halve(layer, s, 1, k)
        kept[1][k][layer, s] = before[home] + arrived[home]

    def third(layer, s, k):
        low, high = sorted(ORDER[k][2:])
        flights[s, k].wait_recv()
        quad[k][layer, s] = kept[1][k][layer, s] + got[1][k][layer, s]
        blocks = ((1 - bits[low], bits[high]), (bits[low], 1 - bits[high]), (1 - bits[low], 1 - bits[high]))
        flights[s, k] = [
            remote(
                quad[k].at[(layer, s, *blocks[i])], pieces[k].at[layer, s, i],
                dx_send.at[layer, s, k, i], dx_recv.at[layer, s, k, i], target,
            )
            for i, target in enumerate(ring(low, high))
        ]

    inverse = {}

    def spread(layer, s, k, number, index, targets):
        place = (layer, s, *index)
        return [
            remote(
                hid[k].at[place], hid[k].at[place],
                ag_send.at[layer, s, k, number + i], ag_recv.at[layer, s, k, number + i], target,
            )
            for i, target in enumerate(targets)
        ]

    def activate(layer, s, k):
        slot, part = k // 2, k % 2
        low_dim, high_dim = sorted(ORDER[k][2:])
        for copy in flights[s, k]:
            copy.wait_recv()
        final = quad[k][layer, s, bits[low_dim], bits[high_dim]].astype(F32)
        for i in range(3):
            final = final + pieces[k][layer, s, i].astype(F32)
        if k == 0:
            tail = final[:, 2 * MAIN :]
            own_lane = lax.broadcasted_iota(jnp.int32, (ROWS, 128), 1) == 2 * LEFT
            mean = jnp.sum(jnp.where(own_lane, tail, 0.0), axis=1, keepdims=True) / D
            inverse[s] = lax.rsqrt(mean + epsilon)
        place = (layer, s, *bits, slice(None))
        cols = slice(part * MAIN, (part + 1) * MAIN)
        hid[k][(*place, slice(0, MAIN))] = gated(
            layer, slot, cols, final[:, 0:MAIN], final[:, MAIN : 2 * MAIN], inverse[s]
        )
        if part == 0:
            tail = final[:, 2 * MAIN :]
            turned = pltpu.roll(tail, 128 - LEFT, 1)
            hid[k][(*place, slice(MAIN, MAIN + 128))] = jnp.zeros((ROWS, 128), BF16)
            hid[k][(*place, slice(MAIN, MAIN + LEFT))] = gated(
                layer, slot, slice(2 * MAIN, FFD), tail[:, 0:LEFT], turned[:, 0:LEFT], inverse[s]
            )
        near = ring(low_dim, high_dim)
        far = ring(*sorted(ORDER[k][:2]))
        flights[s, k] = spread(layer, s, k, 0, bits, near), spread(layer, s, k, 3, bits, far)

    def forward(layer, s, k):
        low, high = sorted(ORDER[k][2:])
        near, far = flights[s, k]
        targets = ring(*sorted(ORDER[k][:2]))
        near[1].wait_recv()
        index = tuple(1 - bits[i] if i == high else bits[i] for i in range(4))
        one = spread(layer, s, k, 6, index, targets)
        near[0].wait_recv()
        near[2].wait_recv()
        index = tuple(1 - bits[i] if i == low else slice(None) if i == high else bits[i] for i in range(4))
        two = spread(layer, s, k, 9, index, targets)
        flights[s, k] = [*far, *one, *two]

    def lower(layer, s):
        for k in CH:
            if k >= 2:
                need(("d", k - 2, layer))
            for copy in flights[s, k]:
                copy.wait_recv()
            part = lax.dot_general(
                drows[k % 2][layer, k // 2],
                hid[k].at[layer, s].reshape(TOK, HID[k])[...],
                (((1,), (1,)), ((), ())),
                preferred_element_type=F32,
            )
            if k == 0:
                total[...] = part
            elif k < 3:
                total[...] += part
            else:
                ypart[layer, s, y] = (total[...] + part).astype(BF16)
        flights[s] = [
            remote(
                ypart.at[layer, s, y], ypart.at[layer, s, y],
                y_send.at[layer, s, i], y_recv.at[layer, s, i], target,
            )
            for i, target in enumerate(ymates)
        ]

    def close(layer, s, scale):
        for copy in flights[s]:
            copy.wait_recv()
        branch = ypart[layer, s, 0].astype(F32)
        for i in range(1, 4):
            branch = branch + ypart[layer, s, i].astype(F32)
        stream[s] = (residual_keep * stream[s].astype(F32) + branch * scale).astype(BF16)

    loads["gain"].wait()
    for layer in range(LAYERS):
        if layer == 0:
            for s in ST:
                loads[("x", s)].wait()
                prepare(0, s)
            cast_up(0)
            pl.semaphore_wait(barrier, len(greet))
            for i in range(2):
                give(("w", i, 0), wcols[i].at[0, 0], wcols[i].at[0, 1], i)
            turns = [(s, k) for half in ((0, 1), (2, 3)) for s in ST for k in half]
            for s, k in turns:
                first(0, s, k)
            for s, k in turns:
                own_half(0, s, k)
            for i in range(6):
                loads[("p", i)].wait()
                give(("p", i), params[i].at[0], params[i].at[1], 8 + i)
            cast_down(0)
            for i in range(2):
                give(("d", i, 0), drows[i].at[0, 0], drows[i].at[0, 1], 4 + i)
            loads["ds"].wait()
        else:
            turns = [(s, k) for s in ST for k in CH]
            for s in ST:
                close(0, s, scale)
                prepare(1, s)
                for k in CH:
                    first(1, s, k)
            for s, k in turns:
                own_half(1, s, k)
        scale = jnp.transpose(jnp.broadcast_to(dscale[layer : layer + 1, :], (TOK, W)))
        for s, k in turns:
            second(layer, s, k)
        if layer == 0:
            cast_up(1)
            for i in range(2):
                give(("w", i, 1), wcols[i].at[1, 0], wcols[i].at[1, 1], 2 + i)
        for s, k in turns:
            third(layer, s, k)
        if layer == 0:
            cast_down(1)
            for i in range(2):
                give(("d", i, 1), drows[i].at[1, 0], drows[i].at[1, 1], 6 + i)
            for i in range(6):
                need(("p", i))
        for s, k in turns:
            activate(layer, s, k)
        for s, k in turns:
            forward(layer, s, k)
        for s in ST:
            lower(layer, s)
    ends = []
    for s in ST:
        close(1, s, scale)
        here = pl.ds(pl.multiple_of(c * 256 + s * TOK, TOK), TOK)
        mine = pltpu.make_async_copy(stream.at[s], out.at[:, here], out_sem.at[s])
        mine.start()
        ends.append((mine, remote(stream.at[s], out.at[:, here], out_sem.at[2 + s], out_sem.at[4 + s], peer)))
    for mine, theirs in ends:
        mine.wait()
        theirs.wait_recv()
    for copy in sent:
        copy.wait_send()


def shards(tokens, norm_gain, gate_weight, gate_scale, value_weight, value_scale, gate_conv, value_conv, *rest):
    gate_bias, value_bias, down_weight, down_scale = rest
    vm = pltpu.VMEM
    dma = pltpu.SemaphoreType.DMA
    lead = (LAYERS, STREAMS)
    scratch = [
        vm((STREAMS, W, TOK), BF16),
        vm((STREAMS, 2, 2, 2, 2, ROWS, 128), F32),
        vm((STREAMS, 2, 2, 2, 2, ROWS, W), F32),
        vm((LAYERS, W), F32),
        vm((LAYERS, W), F32),
        vm((LAYERS, 2, W, FFD), F32),
        vm((LAYERS, W, FFD), F32),
        *(vm((LAYERS, 2, W, PRE[i]), BF16) for i in range(2)),
        *(vm((LAYERS, 2, W, HID[i]), BF16) for i in range(2)),
        *(vm((2, LAYERS, FFD), F32) for _ in range(2)),
        *(vm((2, TAPS, LAYERS, FFD), F32) for _ in range(2)),
        *(vm((2, LAYERS, FFD), F32) for _ in range(2)),
    ]
    for _ in range(3):
        for step in range(2):
            for k in CH:
                scratch.append(vm((*lead, *(2,) * (3 - step), ROWS, PRE[k]), BF16))
    scratch += [vm((*lead, 2, 2, ROWS, PRE[k]), BF16) for k in CH]
    scratch += [vm((*lead, 3, ROWS, PRE[k]), BF16) for k in CH]
    scratch += [vm((*lead, 2, 2, 2, 2, ROWS, HID[k]), BF16) for k in CH]
    scratch += [vm((W, TOK), F32), vm((*lead, 4, W, TOK), BF16)]
    scratch += [
        dma((16,)), dma((16,)), dma((16,)),
        dma((*lead, 2, 4)), dma((*lead, 2, 4)),
        dma((*lead, 4, 3)), dma((*lead, 4, 3)),
        dma((*lead, 4, 12)), dma((*lead, 4, 12)),
        dma((*lead, 3)), dma((*lead, 3)), dma((6,)),
    ]
    result = pl.pallas_call(
        kernel,
        out_shape=jax.ShapeDtypeStruct((W, tokens.shape[0]), BF16),
        in_specs=[pl.BlockSpec(memory_space=pl.ANY)] * 12,
        out_specs=pl.BlockSpec(memory_space=pl.ANY),
        scratch_shapes=scratch,
        compiler_params=pltpu.CompilerParams(
            collective_id=0, has_side_effects=True, vmem_limit_bytes=60 * 1024 * 1024
        ),
        name="two_layers",
    )(
        tokens.T, norm_gain, gate_weight, gate_scale, value_weight, value_scale,
        gate_conv.transpose(1, 0, 2), value_conv.transpose(1, 0, 2), gate_bias, value_bias,
        down_weight.transpose(0, 2, 1), down_scale,
    )
    return result.T


def solution(mesh):
    placed = (
        P(None, "ra"),
        P(None, "ra"),
        P(None, "ra", "cb"),
        P(None, "cb"),
        P(None, "ra", "cb"),
        P(None, "cb"),
        P(None, None, "cb"),
        P(None, None, "cb"),
        P(None, "cb"),
        P(None, "cb"),
        P(None, "cb", "ra"),
        P(None, "ra"),
    )
    return jax.shard_map(
        shards, mesh=mesh, in_specs=placed, out_specs=P(None, "ra"), check_vma=False
    )
```

time: 106 us -> 77.7 us (0.73)
  Pallas kernels: 97 us -> 75.9 us
  local copies, waits for them, and re-layouts: 9.16 us -> 1.62 us
    pallas_call x1, Pallas kernels: 97 us -> 75.9 us  [shards(): pl.pallas_call(kernel, out_shape=jax.ShapeDtypeStruct((W, tokens.shape[0]...]
    unnamed x4 -> x1, local copies, waits for them, and re-layouts: 7.41 us -> 1.62 us
    reshape x1 -> x0, local copies, waits for them, and re-layouts: 1.75 us -> none  [shards(): return result.reshape(count, W)]
where the time goes in v2:
time: 77.7 us; the launch traced here: 77.5 us
  Pallas kernels  75.9 us (98%)
  local copies, waits for them, and re-layouts  1.62 us (2%)
    pallas_call x1, Pallas kernels, shards(): pl.pallas_call(kernel, out_shape=jax.ShapeDtypeStruct((W, tokens.shape[0]...  75.9 us
    unnamed x1, local copies, waits for them, and re-layouts  1.62 us

profile of v2, /device:TPU:1, one launch (start us, length us, event | category | flops | bytes accessed | tf_op | source)
XLA Modules:
  0.0 77.5 jit_solution(3340774480754782455)
XLA Ops:
  0.0 75.9 %two_layers.1 = bf16[192,512]{1,0:T(8,128)(2,1)} custom-call(bf16[192,512]{1,0:T(8,128)(2,1)} %bitcast.7, f32[2,192]{1,0:T(2,128)} %norm_gain.1, f32[2,192,1056]{2,1,0:T(8,128)} %gate_weight.1, f32[2,1056]{1,0:T(2,128)} %gate_scale.1, f32[2,192,1056]{2,1,0:T(8,128)} %value_weight.1, f32[2,1056]{1,0:T(2,128)} %value_scale.1, f32[3,2,1056]{2,1,0:T(2,128)} %bitcast.8, ...), custom_call_target="tpu_custom_call" | custom-call | tf_op jit(solution)/shard_map/two_layers/pallas_call | solution.py:429
  75.9 1.6 %copy.14 = bf16[512,192]{0,1:T(8,128)(2,1)} copy(bf16[512,192]{0,1:T(8,128)(2,1)} %bitcast.6) | data formatting | bytes 393216
